TPU v7x, 512 devices: a whole 4x8x8 slice. The times are simulated.
512 devices in a mesh: ep: 32 (over z, x), tp: 16 (over y, core).
Axes of the slice: x: 4, y: 8, z: 8, core: 2. Of those that a mesh axis runs over, the one named last changes fastest.
Arguments:
- mixer_query: bfloat16 [8192, 2048], P('ep', 'tp'), may hold values from -6 to 6
- mixer_forget: bfloat16 [8192, 2048], P('ep', 'tp'), may hold values from -5.5 to 5.5
- mixer_value: bfloat16 [8192, 2048], P('ep', 'tp'), may hold values from -6 to 6
- mixer_gate: bfloat16 [8192, 2048], P('ep', 'tp'), may hold values from -6 to 6
- forget_floor: float32 [2048], P('tp'), may hold values from 0.88 to 1
- head_gain: float32 [128], replicated, may hold values from 0.1 to 1.9
- mixer_proj: bfloat16 [2048, 2048], P(None, 'tp'), may hold values from -0.125 to 0.125
- expert_tokens: bfloat16 [4096, 2048], P('ep'), may hold values from -6 to 6
- expert_gain: float32 [2048], replicated, may hold values from 0.1 to 1.9
- routes: int32 [4096, 2], P('ep'), may hold values from 0 to 31, as said below
- group_logits: float32 [4096, 4], P('ep'), may hold values from -6 to 6
- choice_logits: float32 [4096, 2], P('ep'), may hold values from -6 to 6
- w_gate: bfloat16 [32, 2048, 2048], P('ep', None, 'tp'), may hold values from -0.125 to 0.125
- w_up: bfloat16 [32, 2048, 2048], P('ep', None, 'tp'), may hold values from -0.125 to 0.125
- w_down: bfloat16 [32, 2048, 2048], P('ep', None, 'tp'), may hold values from -0.125 to 0.125
Outputs:
- mixer_out: bfloat16 [8192, 2048], P('ep', 'tp')
- expert_out: bfloat16 [4096, 2048], P('ep', 'tp')
Inputs may be any that keep to these rules, and one draw needn't show every extreme that they name: `routes`: in each aligned block of 128 rows (the rows of one index of ep) no expert is named by more than 16 rows, and some expert reaches that bound in every block; the 2 experts of a row differ and lie in the same group.
All inputs are finite; a program needn't handle non-finite values.
Results may differ from a plain program's by a relative error of at most 0.01.
Values may be sent and summed in bfloat16 or wider, within the bound.
A program may use at most 64 MiB of HBM per device.

v0:
```python
import jax
import jax.numpy as jnp
from jax import lax
from jax.sharding import Mesh
from jax.sharding import PartitionSpec as P

KEYDIM = 128
VDIM = 128
GROUPS = 4
TOPK = 2
BLOCK = 64
EP = ("ep_0", "ep_1")
norm_eps = 1e-06
highest_precision = lax.Precision.HIGHEST


def filled_with(shard, identity):
    return jax.tree.map(
        lambda part, zero: jnp.zeros_like(part) + jnp.asarray(zero, part.dtype), shard, identity
    )


def collected_together(shard, axis):
    leaves = jax.tree.leaves(shard)
    sequence = sorted(range(len(leaves)), key=lambda k: -leaves[k].size)
    width = (1, *leaves[sequence[0]].shape)[-1]
    lines = [
        jnp.pad(leaves[k].reshape(-1), (0, -leaves[k].size % width)).reshape(-1, width)
        for k in sequence
    ]
    both, at, found = (lax.all_gather(jnp.concatenate(lines), axis), 0, {})
    for k, line in zip(sequence, lines):
        section = both[:, at : at + len(line)].reshape(len(both), -1)
        found[k] = section[:, : leaves[k].size].reshape(-1, *leaves[k].shape)
        at += len(line)
    numbers = iter(range(len(leaves)))
    return jax.tree.map(lambda _: found[next(numbers)], shard)


def carried_in(shard, axes, combine, identity):
    before = start = filled_with(shard, identity)
    so_far = shard
    for axis in reversed(axes):
        devices, index = (lax.axis_size(axis), lax.axis_index(axis))
        pieces = collected_together(
            jax.tree.map(
                lambda part, kind: part.astype(kind), so_far, (jnp.bfloat16, jnp.bfloat16)
            ),
            axis,
        )
        inside, so_far = (start, start)
        for k in range(devices):
            passed = k < index
            so_far = combine(
                so_far, jax.tree.map(lambda part, own: part[k].astype(own.dtype), pieces, shard)
            )
            inside = jax.tree.map(lambda new, old: jnp.where(passed, new, old), so_far, inside)
        before = combine(inside, before)
    return before


def laid_out(pieces, dim):
    dims = list(pieces.shape[1:])
    dims[dim] *= pieces.shape[0]
    return jnp.moveaxis(pieces, 0, dim).reshape(dims)


def from_everyone(shard, axis):
    copies = jnp.broadcast_to(shard, (lax.axis_size(axis), *shard.shape))
    return lax.all_to_all(copies, axis, split_axis=0, concat_axis=0, tiled=True)


def gather_directly(shard, axis, dim):
    return laid_out(from_everyone(shard, axis), dim)


def rms_scale(features, gain_vec):
    return (
        features
        * lax.rsqrt(jnp.mean(features * features, axis=-1, keepdims=True) + norm_eps)
        * gain_vec
    )


def block_terms(query_block, input_block, log_blk, value_block, carried_state):
    cumulative_log = jnp.cumsum(log_blk, axis=0)
    between_block_term = jnp.einsum(
        "zug,ugr->zur",
        query_block * jnp.exp(cumulative_log),
        carried_state,
        precision=highest_precision,
    )
    causal = jnp.tril(jnp.ones((query_block.shape[0], query_block.shape[0]), dtype=bool))[
        :, :, None, None
    ]
    differ = cumulative_log[:, None] - cumulative_log[None, :]
    decays = jnp.exp(jnp.where(causal, differ, -jnp.inf))
    scores = jnp.sum(query_block[:, None] * input_block[None, :] * decays, axis=-1)
    result = between_block_term + jnp.einsum(
        "tsh,shv->thv", scores, value_block, precision=highest_precision
    )
    ending_log_decay = cumulative_log[-1]
    updated_state = jnp.exp(ending_log_decay)[..., None] * carried_state + jnp.einsum(
        "twa,twr->war",
        input_block * jnp.exp(ending_log_decay[None] - cumulative_log),
        value_block,
        precision=highest_precision,
    )
    return (updated_state, result, cumulative_log)


def mixer_local(
    mixer_query, mixer_forget, mixer_value, mixer_gate, forget_floor, head_gain, mixer_proj
):
    length = mixer_query.shape[0]
    heads_local = mixer_query.shape[1] // KEYDIM
    blocks = length // BLOCK

    def split_blocks(source_array, last_width):
        return source_array.reshape(blocks, BLOCK, heads_local, last_width)

    queries = jax.nn.silu(mixer_query.astype(jnp.float32))
    input_rates = (1.0 - forget_floor) * jax.nn.sigmoid(-mixer_forget.astype(jnp.float32))
    log_forget = jnp.log1p(-input_rates)
    value_rows = mixer_value.astype(jnp.float32)

    def advance(carry_pair, block_inputs):
        carried_state, offset_log = carry_pair
        query_block, input_block, value_block, log_blk = block_inputs
        updated_state, result, cumulative_log = block_terms(
            query_block, input_block, log_blk, value_block, carried_state
        )
        scaled_values = query_block * jnp.exp(cumulative_log + offset_log[None])
        return ((updated_state, offset_log + cumulative_log[-1]), (result, scaled_values))

    initial = (
        jnp.zeros((heads_local, KEYDIM, VDIM), jnp.float32),
        jnp.zeros((heads_local, KEYDIM), jnp.float32),
    )
    (local_state, total_log), (output_rows, scaled_values) = lax.scan(
        advance,
        initial,
        (
            split_blocks(queries, KEYDIM),
            split_blocks(input_rates, KEYDIM),
            split_blocks(value_rows, VDIM),
            split_blocks(log_forget, KEYDIM),
        ),
    )

    def combine(earlier, later):
        return (earlier[0] * later[0], later[0][..., None] * earlier[1] + later[1])

    identity = (jnp.ones_like(total_log), jnp.zeros_like(local_state))
    incoming_state = carried_in((jnp.exp(total_log), local_state), EP, combine, identity)
    output_rows = output_rows + jnp.einsum(
        "qsfa,fap->qsfp", scaled_values, incoming_state[1], precision=highest_precision
    )
    output_rows = output_rows.reshape(length, heads_local, VDIM)
    gate_act = jax.nn.silu(mixer_gate.astype(jnp.float32)).reshape(length, heads_local, VDIM)
    gated_out = rms_scale(output_rows, head_gain) * gate_act
    mixed_heads = gated_out.reshape(length, heads_local * VDIM).astype(jnp.bfloat16)
    summed = jnp.dot(
        lax.all_gather(mixed_heads, "tp", axis=1, tiled=True),
        mixer_proj,
        preferred_element_type=jnp.float32,
    )
    return summed.astype(jnp.bfloat16)


def gate_weights(routes, group_logits, choice_logits, group_size):
    group_exp = jnp.exp(group_logits)
    group_prob = group_exp / jnp.sum(group_exp, axis=-1, keepdims=True)
    groups_of = routes // group_size
    member = (groups_of[..., None] == jnp.arange(GROUPS, dtype=jnp.int32)).astype(jnp.float32)
    picked_prob = jnp.sum(member * group_prob[:, None, :], axis=-1)
    choice_exp = jnp.exp(choice_logits)
    together = (groups_of[:, :, None] == groups_of[:, None, :]).astype(jnp.float32)
    within = jnp.sum(together * choice_exp[:, None, :], axis=-1)
    return picked_prob * choice_exp / within


def finish(gate_pre, up_pre, down_local, sources, slot_count):
    hidden = (jax.nn.silu(gate_pre) * up_pre).astype(jnp.bfloat16)
    summed = jnp.dot(
        gather_directly(hidden, "tp", 1), down_local, preferred_element_type=jnp.float32
    )
    shaped = summed.astype(jnp.bfloat16).reshape(sources, slot_count, down_local.shape[1])
    return lax.all_to_all(shaped, EP, split_axis=0, concat_axis=0, tiled=True)


def expert_local(
    expert_tokens, expert_gain, routes, group_logits, choice_logits, w_gate, w_up, w_down
):
    count_rows, model_width = expert_tokens.shape
    experts_all = lax.axis_size(EP)
    capacity = 2 * TOPK * count_rows // experts_all
    normed = rms_scale(expert_tokens.astype(jnp.float32), expert_gain).astype(jnp.bfloat16)
    weights = gate_weights(routes, group_logits, choice_logits, experts_all // GROUPS)
    flat_routes = routes.reshape(-1)
    onehot = (flat_routes[:, None] == jnp.arange(experts_all, dtype=jnp.int32)).astype(jnp.int32)
    earlier = jnp.cumsum(onehot, axis=0) - onehot
    ranks = jnp.sum(earlier * onehot, axis=-1)
    slot_of = flat_routes * capacity + ranks
    token_ids = jnp.arange(flat_routes.shape[0], dtype=jnp.int32) // TOPK
    token_of = jnp.full((experts_all * capacity,), count_rows, jnp.int32).at[slot_of].set(token_ids)
    padded = jnp.concatenate([normed, jnp.zeros((1, model_width), jnp.bfloat16)], axis=0)
    outgoing = padded[token_of].reshape(experts_all, capacity, model_width)
    gate_local = w_gate[0]
    up_local = w_up[0]
    down_local = w_down[0]
    arrived = lax.all_to_all(outgoing, EP, split_axis=0, concat_axis=0, tiled=True)
    sources, slot_count, _ = arrived.shape
    flat_in = arrived.reshape(sources * slot_count, model_width)
    gate_pre = jnp.dot(flat_in, gate_local, preferred_element_type=jnp.float32)
    up_pre = jnp.dot(flat_in, up_local, preferred_element_type=jnp.float32)
    came_back = finish(gate_pre, up_pre, down_local, sources, slot_count)
    picked = (
        came_back.reshape(-1, came_back.shape[-1])[slot_of].astype(jnp.float32)
        * weights.reshape(-1)[:, None]
    )
    return jnp.sum(picked.reshape(count_rows, TOPK, -1), axis=1).astype(jnp.bfloat16)


def per_device(
    mixer_query,
    mixer_forget,
    mixer_value,
    mixer_gate,
    forget_floor,
    head_gain,
    mixer_proj,
    expert_tokens,
    expert_gain,
    routes,
    group_logits,
    choice_logits,
    w_gate,
    w_up,
    w_down,
):
    mixer_out = mixer_local(
        mixer_query, mixer_forget, mixer_value, mixer_gate, forget_floor, head_gain, mixer_proj
    )
    expert_out = expert_local(
        expert_tokens, expert_gain, routes, group_logits, choice_logits, w_gate, w_up, w_down
    )
    return (mixer_out, expert_out)


def solution(mesh):
    finer = Mesh(mesh.devices.reshape(8, 4, mesh.shape["tp"]), ("ep_0", "ep_1", "tp"))
    placed = (
        P(EP, "tp"),
        P(EP, "tp"),
        P(EP, "tp"),
        P(EP, "tp"),
        P("tp"),
        P(),
        P(None, "tp"),
        P(EP, None),
        P(),
        P(EP, None),
        P(EP, None),
        P(EP, None),
        P(EP, None, "tp"),
        P(EP, None, "tp"),
        P(EP, None, "tp"),
    )
    return jax.shard_map(
        per_device,
        mesh=finer,
        in_specs=placed,
        out_specs=(P(EP, "tp"), P(EP, "tp")),
        check_vma=False,
    )
```

profile of v0, /device:TPU:1, one launch (start us, length us, event | category | flops | bytes accessed | tf_op | source)
XLA Modules:
  0.0 173.8 jit_solution(17011988294751444505)
XLA Ops:
  7.2 0.8 copy.50
  8.3 0.7 and_select_fusion
  10.2 1.4 scatter_custom_fusion
  11.6 1.2 fusion.24
  12.9 1.2 fusion.26
  14.2 3.3 %gather_fusion = bf16[512,2048]{1,0:T(8,128)(2,1)} fusion(bf16[129,2048]{1,0:T(8,128)(2,1)S(1)} %concatenate.11, s32[1024]{0:T(1024)S(1)} %pad_clamp_fusion.1), kind=kCustom, calls=%fused_computation | custom fusion | bytes 4196352 | tf_op jit(solution)/shard_map/gather | solution.py:208
  17.5 13.8 %all-to-all-start = ((bf16[32,16,2048]{2,1,0:T(8,128)(2,1)}), bf16[32,16,2048]{2,1,0:T(8,128)(2,1)S(1)}, u32[]{:S(2)}, u32[]{:S(2)}) async-start(bf16[32,16,2048]{2,1,0:T(8,128)(2,1)} %bitcast.31), calls=%async_computation | async-start | bytes 4194304 | tf_op jit(solution)/shard_map/all_to_all | solution.py:212
  31.6 13.7 %while.17 = (s32[]{:T(128)}, f32[1,128,128]{2,1,0:T(8,128)S(1)}, f32[1,128]{1,0:T(1,128)S(1)}, f32[4,64,1,128]{3,1,2,0:T(8,128)}, f32[4,64,1,128]{3,1,2,0:T(8,12...) while((s32[]{:T(128)}, f32[1,128,128]{2,1,0:T(8,128)S(1)}, ...), condition=%wide.region_3.4_spmd.clone, body=%wide.region_0.3_spmd.clone.sunk | while | flops 34709760 | bytes 1030797 | solution.py:140
  32.4 1.4 multiply_reduce_fusion.3
  34.0 0.8 fusion.173
  35.8 1.4 multiply_reduce_fusion.3
  37.4 0.8 fusion.173
  39.2 1.4 multiply_reduce_fusion.3
  40.8 0.8 fusion.173
  42.7 1.4 multiply_reduce_fusion.3
  44.2 0.8 fusion.173
  45.4 10.6 %all-gather.2 = bf16[4,129,128]{2,1,0:T(8,128)(2,1)S(1)} all-gather(bf16[1,129,128]{2,1,0:T(8,128)(2,1)S(1)} %maximum_bitcast_fusion), channel_id=2, replica_groups=mesh['ep_0'=8,'ep_1'=4,'tp'=16] {'ep_1'}, dimensions={0}, use_global_device_ids=true | all-gather | bytes 165120 | tf_op jit(solution)/shard_map/all_gather | solution.py:31
  56.0 23.8 %all-to-all-done = bf16[32,16,2048]{2,1,0:T(8,128)(2,1)S(1)} async-done(((bf16[32,16,2048]{2,1,0:T(8,128)(2,1)}), bf16[32,16,2048]{2,1,0:T(8,128)(2,1)S(1)}, u32[]{:S(2)}, u32[]{:S(2)}) %all-to-all-start) | async-done | bytes 2097184 | tf_op jit(solution)/shard_map/all_to_all | solution.py:212
  79.9 0.7 fusion.29
  80.6 0.7 fusion.22
  81.4 1.6 broadcast_in_dim.37
  83.0 9.9 %all-to-all-start.1 = ((bf16[16,512,128]{1,2,0:T(8,128)(2,1)}), bf16[16,512,128]{1,2,0:T(8,128)(2,1)S(1)}, u32[]{:S(2)}, u32[]{:S(2)}) async-start(bf16[16,512,128]{1,2,0:T(8,128)(2,1)} %broadcast_in_dim.37), calls=%async_computation.1 | async-start | bytes 4194304 | tf_op jit(solution)/shard_map/all_to_all | solution.py:70
  93.1 20.6 %all-gather.3 = bf16[8,129,128]{2,1,0:T(8,128)(2,1)S(1)} all-gather(bf16[1,129,128]{2,1,0:T(8,128)(2,1)S(1)} %maximum_bitcast_fusion.1), channel_id=3, replica_groups=mesh['ep_0'=8,'ep_1'=4,'tp'=16] {'ep_0'}, dimensions={0}, use_global_device_ids=true | all-gather | bytes 297216 | tf_op jit(solution)/shard_map/all_gather | solution.py:31
  113.8 1.7 multiply_reduce_fusion.1
  115.6 0.7 fusion.41
  116.6 26.2 %all-to-all-done.1 = bf16[16,512,128]{1,2,0:T(8,128)(2,1)S(1)} async-done(((bf16[16,512,128]{1,2,0:T(8,128)(2,1)}), bf16[16,512,128]{1,2,0:T(8,128)(2,1)S(1)}, u32[]{:S(2)}, u32[]{:S(2)}) %all-to-all-start.1) | async-done | bytes 2097184 | tf_op jit(solution)/shard_map/all_to_all | solution.py:70
  142.8 2.4 %convolution_convert_fusion = bf16[512,128]{1,0:T(8,128)(2,1)} fusion(bf16[512,2048]{0,1:T(8,128)(2,1)S(1)} %bitcast.225, bf16[1,2048,128]{2,1,0:T(8,128)(2,1)} %param.31), kind=kOutput, calls=%fused_computation.42 | convolution fusion | flops 268500992 | bytes 2752512 | tf_op jit(solution)/shard_map/dot_general | solution.py:185
  145.2 5.1 %all-to-all-start.2 = ((bf16[32,16,128]{2,1,0:T(8,128)(2,1)}), bf16[32,16,128]{2,1,0:T(8,128)(2,1)S(1)}, u32[]{:S(2)}, u32[]{:S(2)}) async-start(bf16[32,16,128]{2,1,0:T(8,128)(2,1)} %bitcast.38), calls=%async_computation.2 | async-start | bytes 262144 | tf_op jit(solution)/shard_map/all_to_all | solution.py:189
  150.3 12.6 %all-gather.6.cloned.1.call-done = bf16[256,2048]{1,0:T(8,128)(2,1)} async-done(((bf16[256,128]{1,0:T(8,128)(2,1)}), bf16[256,2048]{1,0:T(8,128)(2,1)}) %all-gather.6.cloned.1.call-update) | async-done | bytes 1048592 | tf_op jit(solution)/shard_map/all_gather | solution.py:164
  162.9 2.3 %convolution_convert_fusion.1 = bf16[256,128]{1,0:T(8,128)(2,1)} fusion(bf16[256,2048]{1,0:T(8,128)(2,1)} %all-gather.6.cloned.1.call-done, bf16[2048,128]{1,0:T(8,128)(2,1)S(1)} %copy-done.1), kind=kOutput, calls=%fused_computation.45 | convolution fusion | flops 134250496 | bytes 1638400 | tf_op jit(solution)/shard_map/dot_general | solution.py:163
  165.2 0.9 gather_fusion.1
  166.1 0.9 fusion.38
  (114 shorter events, 7.3 us)
Async XLA Ops:
  7.2 72.7 %copy-start = (bf16[1,2048,128]{2,1,0:T(8,128)(2,1)S(1)}, bf16[1,2048,128]{2,1,0:T(8,128)(2,1)}, u32[]{:S(2)}) copy-start(bf16[1,2048,128]{2,1,0:T(8,128)(2,1)} %param.29) | copy-start | bytes 1572868
  17.5 13.9 %copy-start.10 = (f32[128]{0:T(128)S(1)}, f32[128]{0:T(128)}, u32[]{:S(2)}) copy-start(f32[128]{0:T(128)} %param.21) | copy-start | bytes 1540
  17.5 13.9 %copy-start.2 = (bf16[256,128]{1,0:T(8,128)(2,1)S(1)}, bf16[256,128]{1,0:T(8,128)(2,1)}, u32[]{:S(2)}) copy-start(bf16[256,128]{1,0:T(8,128)(2,1)} %param.19) | copy-start | bytes 196612
  17.5 14.0 %copy-start.3 = (bf16[256,128]{1,0:T(8,128)(2,1)S(1)}, bf16[256,128]{1,0:T(8,128)(2,1)}, u32[]{:S(2)}) copy-start(bf16[256,128]{1,0:T(8,128)(2,1)} %param.17) | copy-start | bytes 196612
  17.5 14.0 %copy-start.4 = (bf16[256,128]{1,0:T(8,128)(2,1)S(1)}, bf16[256,128]{1,0:T(8,128)(2,1)}, u32[]{:S(2)}) copy-start(bf16[256,128]{1,0:T(8,128)(2,1)} %param.18) | copy-start | bytes 196612
  17.5 62.3 %all-to-all-start = ((bf16[32,16,2048]{2,1,0:T(8,128)(2,1)}), bf16[32,16,2048]{2,1,0:T(8,128)(2,1)S(1)}, u32[]{:S(2)}, u32[]{:S(2)}) async-start(bf16[32,16,2048]{2,1,0:T(8,128)(2,1)} %bitcast.31), calls=%async_computation | async-start | bytes 4194304 | tf_op jit(solution)/shard_map/all_to_all | solution.py:212
  45.4 35.2 %copy-start.9 = (bf16[1,2048,128]{2,1,0:T(8,128)(2,1)S(1)}, bf16[1,2048,128]{2,1,0:T(8,128)(2,1)}, u32[]{:S(2)}) copy-start(bf16[1,2048,128]{2,1,0:T(8,128)(2,1)} %param.30) | copy-start | bytes 1572868
  83.0 32.6 %copy-start.5 = (bf16[256,128]{1,0:T(8,128)(2,1)S(1)}, bf16[256,128]{1,0:T(8,128)(2,1)}, u32[]{:S(2)}) copy-start(bf16[256,128]{1,0:T(8,128)(2,1)} %param.20) | copy-start | bytes 196612
  83.0 32.6 %copy-start.8 = (f32[128]{0:T(128)S(1)}, f32[128]{0:T(128)}, u32[]{:S(2)}) copy-start(f32[128]{0:T(128)} %param.22) | copy-start | bytes 1540
  83.0 59.8 %all-to-all-start.1 = ((bf16[16,512,128]{1,2,0:T(8,128)(2,1)}), bf16[16,512,128]{1,2,0:T(8,128)(2,1)S(1)}, u32[]{:S(2)}, u32[]{:S(2)}) async-start(bf16[16,512,128]{1,2,0:T(8,128)(2,1)} %broadcast_in_dim.37), calls=%async_computation.1 | async-start | bytes 4194304 | tf_op jit(solution)/shard_map/all_to_all | solution.py:70
  92.9 23.5 %copy-start.7 = (f32[128,2]{0,1:T(2,128)S(1)}, f32[128,2]{0,1:T(2,128)}, u32[]{:S(2)}) copy-start(f32[128,2]{0,1:T(2,128)} %param.28) | copy-start | bytes 3076
  92.9 23.5 %copy-start.6 = (f32[128,4]{0,1:T(4,128)S(1)}, f32[128,4]{0,1:T(4,128)}, u32[]{:S(2)}) copy-start(f32[128,4]{0,1:T(4,128)} %param.27) | copy-start | bytes 6148
  92.9 70.0 %all-gather.6.cloned.1.call-start = ((), (), s32[]{:S(2)}) async-start(), calls=%async_computation.3 | async-start | bytes 1114112 | tf_op jit(solution)/shard_map/all_gather | solution.py:164
  113.8 49.2 %copy-start.1 = (bf16[2048,128]{1,0:T(8,128)(2,1)S(1)}, bf16[2048,128]{1,0:T(8,128)(2,1)}, u32[]{:S(2)}) copy-start(bf16[2048,128]{1,0:T(8,128)(2,1)} %param.23) | copy-start | bytes 1572868
  145.2 20.0 %all-to-all-start.2 = ((bf16[32,16,128]{2,1,0:T(8,128)(2,1)}), bf16[32,16,128]{2,1,0:T(8,128)(2,1)S(1)}, u32[]{:S(2)}, u32[]{:S(2)}) async-start(bf16[32,16,128]{2,1,0:T(8,128)(2,1)} %bitcast.38), calls=%async_computation.2 | async-start | bytes 262144 | tf_op jit(solution)/shard_map/all_to_all | solution.py:189
Sparse Core Ops, SparseCore 0:
  116.4 46.4 all-gather.5
where the time goes:
time: 174 us
  waiting for transfers between devices  62.6 us (36%)
  blocking collectives  31.2 us (18%)
  starting transfers between devices  28.9 us (17%)
  between operations  14.4 us (8%)
  other arithmetic  14.2 us (8%)
  matrix products  12.9 us (7%)
  local copies, waits for them, and re-layouts  9.24 us (5%)
    all_gather x2, blocking collectives, collected_together(): both, at, found = (lax.all_gather(jnp.concatenate(lines), axis), 0, {})  31.2 us
    all_to_all x1, waiting for transfers between devices, from_everyone(): return lax.all_to_all(copies, axis, split_axis=0, concat_axis=0, tiled=True)  26.2 us
    all_to_all x1, waiting for transfers between devices, expert_local(): lax.all_to_all(outgoing, EP, split_axis=0, concat_axis=0, tiled=True)  23.8 us
    all_to_all x1, starting transfers between devices, expert_local(): lax.all_to_all(outgoing, EP, split_axis=0, concat_axis=0, tiled=True)  13.8 us
    all_gather x1, waiting for transfers between devices, mixer_local(): lax.all_gather(mixed_heads, 'tp', axis=1, tiled=True)  12.6 us
    all_to_all x1, starting transfers between devices, from_everyone(): return lax.all_to_all(copies, axis, split_axis=0, concat_axis=0, tiled=True)  9.89 us
    reduce_sum x4, other arithmetic, block_terms(): jnp.sum(query_block[:, None] * input_block[None, :] * decays, axis=-1)  5.4 us
    all_to_all x1, starting transfers between devices, finish(): return lax.all_to_all(shaped, EP, split_axis=0, concat_axis=0, tiled=True)  5.08 us
  transfers between devices with their start and end apart: 4, of which 3 were waited for; matrix products, arithmetic and copies ran while one was open for 12% of the time, Pallas kernels for 0%

commit v1 on v0

--- a/solution.py
+++ b/solution.py
@@ -12,6 +12,11 @@
 EP = ("ep_0", "ep_1")
 norm_eps = 1e-06
 highest_precision = lax.Precision.HIGHEST
+
+
+def all_by_exchange(array, name, along):
+    sent = jnp.stack([array] * lax.axis_size(name))
+    return jnp.concatenate(lax.all_to_all(sent, name, 0, 0), axis=along)
 
 
 def filled_with(shard, identity):
@@ -161,9 +166,7 @@
     gated_out = rms_scale(output_rows, head_gain) * gate_act
     mixed_heads = gated_out.reshape(length, heads_local * VDIM).astype(jnp.bfloat16)
     summed = jnp.dot(
-        lax.all_gather(mixed_heads, "tp", axis=1, tiled=True),
-        mixer_proj,
-        preferred_element_type=jnp.float32,
+        all_by_exchange(mixed_heads, "tp", 1), mixer_proj, preferred_element_type=jnp.float32
     )
     return summed.astype(jnp.bfloat16)
 

time: 174 us -> 189 us (1.086)
  waiting for transfers between devices: 62.6 us -> 89.2 us
  between operations: 14.4 us -> 1.04 us
  starting transfers between devices: 28.9 us -> 35.3 us
  matrix products: 12.9 us -> 9.52 us
  other arithmetic: 14.2 us -> 11.2 us
    all_to_all x0 -> x1, waiting for transfers between devices: none -> 25.4 us  [all_by_exchange(): return jnp.concatenate(lax.all_to_all(sent, name, 0, 0), axis=along)]
    all_to_all x1, waiting for transfers between devices: 23.8 us -> 48.2 us  [expert_local(): lax.all_to_all(outgoing, EP, split_axis=0, concat_axis=0, tiled=True)]
    all_to_all x1, waiting for transfers between devices: 26.2 us -> 7.94 us  [from_everyone(): return lax.all_to_all(copies, axis, split_axis=0, concat_axis=0, tiled=True)]
    all_gather x1 -> x0, waiting for transfers between devices: 12.6 us -> none  [mixer_local(): lax.all_gather(mixed_heads, 'tp', axis=1, tiled=True)]
    all_to_all x1, waiting for transfers between devices: 0.01 us -> 7.69 us  [finish(): return lax.all_to_all(shaped, EP, split_axis=0, concat_axis=0, tiled=True)]
    all_to_all x0 -> x1, starting transfers between devices: none -> 5.78 us  [all_by_exchange(): return jnp.concatenate(lax.all_to_all(sent, name, 0, 0), axis=along)]
    dot_general x4, matrix products: 3.09 us -> 0.66 us  [block_terms(): jnp.einsum('tsh,shv->thv', scores, value_block, precision=highest_precision)]
    dynamic_update_slice x4, other arithmetic: 2.49 us -> 0.07 us  [mixer_local(): lax.scan(advance, initial, (split_blocks(queries, KEYDIM), split_blocks(i...]
  transfers between devices with their start and end apart: 4 -> 4, of which waited for: 3 -> 4; matrix products, arithmetic and copies ran while one was open for 12% -> 8% of each run, Pallas kernels for 0% -> 0%
where the time goes in v1:
time: 189 us; the launch traced here: 188 us
  waiting for transfers between devices  89.2 us (47%)
  starting transfers between devices  35.3 us (19%)
  blocking collectives  30.8 us (16%)
  other arithmetic  11.2 us (6%)
  local copies, waits for them, and re-layouts  10.9 us (6%)
  matrix products  9.52 us (5%)
    all_to_all x1, waiting for transfers between devices, expert_local(): lax.all_to_all(outgoing, EP, split_axis=0, concat_axis=0, tiled=True)  48.2 us
    all_gather x2, blocking collectives, collected_together(): both, at, found = (lax.all_gather(jnp.concatenate(lines), axis), 0, {})  30.8 us
    all_to_all x1, waiting for transfers between devices, all_by_exchange(): return jnp.concatenate(lax.all_to_all(sent, name, 0, 0), axis=along)  25.4 us
    all_to_all x1, starting transfers between devices, expert_local(): lax.all_to_all(outgoing, EP, split_axis=0, concat_axis=0, tiled=True)  13.8 us
    all_to_all x1, starting transfers between devices, from_everyone(): return lax.all_to_all(copies, axis, split_axis=0, concat_axis=0, tiled=True)  9.89 us
    all_to_all x1, waiting for transfers between devices, from_everyone(): return lax.all_to_all(copies, axis, split_axis=0, concat_axis=0, tiled=True)  7.94 us
    all_to_all x1, waiting for transfers between devices, finish(): return lax.all_to_all(shaped, EP, split_axis=0, concat_axis=0, tiled=True)  7.69 us
    all_to_all x1, starting transfers between devices, all_by_exchange(): return jnp.concatenate(lax.all_to_all(sent, name, 0, 0), axis=along)  5.78 us
  transfers between devices with their start and end apart: 4, of which 4 were waited for; matrix products, arithmetic and copies ran while one was open for 8% of the time, Pallas kernels for 0%

profile of v1, /device:TPU:1, one launch (start us, length us, event | category | flops | bytes accessed | tf_op | source)
XLA Modules:
  0.0 188.3 jit_solution(12842501978591698539)
XLA Ops:
  0.6 0.8 copy.53
  1.8 0.7 and_select_fusion
  2.5 0.6 reduce-window.6
  3.7 1.4 scatter_custom_fusion
  5.1 1.2 fusion.24
  6.3 1.2 fusion.26
  7.6 3.3 %gather_fusion = bf16[512,2048]{1,0:T(8,128)(2,1)} fusion(bf16[129,2048]{1,0:T(8,128)(2,1)S(1)} %concatenate.11, s32[1024]{0:T(1024)S(1)} %pad_clamp_fusion.1), kind=kCustom, calls=%fused_computation | custom fusion | bytes 4196352 | tf_op jit(solution)/shard_map/gather | solution.py:211
  11.0 13.8 %all-to-all-start.1 = ((bf16[32,16,2048]{2,1,0:T(8,128)(2,1)}), bf16[32,16,2048]{2,1,0:T(8,128)(2,1)S(1)}, u32[]{:S(2)}, u32[]{:S(2)}) async-start(bf16[32,16,2048]{2,1,0:T(8,128)(2,1)} %bitcast.33), calls=%async_computation.1 | async-start | bytes 4194304 | tf_op jit(solution)/shard_map/all_to_all | solution.py:215
  25.1 48.2 %all-to-all-done.1 = bf16[32,16,2048]{2,1,0:T(8,128)(2,1)S(1)} async-done(((bf16[32,16,2048]{2,1,0:T(8,128)(2,1)}), bf16[32,16,2048]{2,1,0:T(8,128)(2,1)S(1)}, u32[]{:S(2)}, u32[]{:S(2)}) %all-to-all-start.1) | async-done | bytes 2097184 | tf_op jit(solution)/shard_map/all_to_all | solution.py:215
  73.3 0.7 fusion.29
  74.0 0.3 copy-done.9
  74.4 0.7 fusion.22
  75.2 1.6 broadcast_in_dim.37
  76.8 9.9 %all-to-all-start.2 = ((bf16[16,512,128]{1,2,0:T(8,128)(2,1)}), bf16[16,512,128]{1,2,0:T(8,128)(2,1)S(1)}, u32[]{:S(2)}, u32[]{:S(2)}) async-start(bf16[16,512,128]{1,2,0:T(8,128)(2,1)} %broadcast_in_dim.37), calls=%async_computation.2 | async-start | bytes 4194304 | tf_op jit(solution)/shard_map/all_to_all | solution.py:75
  86.7 9.0 %while.17 = (s32[]{:T(128)}, f32[1,128,128]{2,1,0:T(8,128)S(1)}, f32[1,128]{1,0:T(1,128)S(1)}, f32[4,64,1,128]{3,1,2,0:T(8,128)S(1)}, f32[4,64,1,128]{3,1,2,0:T(...) while((s32[]{:T(128)}, f32[1,128,128]{2,1,0:T(8,128)S(1)}, ...), condition=%wide.region_3.4_spmd.clone, body=%wide.region_0.3_spmd.clone.sunk | while | flops 34709760 | bytes 1046165 | solution.py:145
  86.8 1.4 multiply_reduce_fusion.3
  89.1 1.4 multiply_reduce_fusion.3
  91.4 1.4 multiply_reduce_fusion.3
  93.6 1.4 multiply_reduce_fusion.3
  95.8 10.2 %all-gather.2 = bf16[4,129,128]{2,1,0:T(8,128)(2,1)S(1)} all-gather(bf16[1,129,128]{2,1,0:T(8,128)(2,1)S(1)} %maximum_bitcast_fusion), channel_id=2, replica_groups=mesh['ep_0'=8,'ep_1'=4,'tp'=16] {'ep_1'}, dimensions={0}, use_global_device_ids=true | all-gather | bytes 165120 | tf_op jit(solution)/shard_map/all_gather | solution.py:36
  106.2 20.5 %all-gather.3 = bf16[8,129,128]{2,1,0:T(8,128)(2,1)S(1)} all-gather(bf16[1,129,128]{2,1,0:T(8,128)(2,1)S(1)} %maximum_bitcast_fusion.1), channel_id=3, replica_groups=mesh['ep_0'=8,'ep_1'=4,'tp'=16] {'ep_0'}, dimensions={0}, use_global_device_ids=true | all-gather | bytes 297216 | tf_op jit(solution)/shard_map/all_gather | solution.py:36
  126.8 0.7 multiply_reduce_fusion.1
  127.8 7.9 %all-to-all-done.2 = bf16[16,512,128]{1,2,0:T(8,128)(2,1)S(1)} async-done(((bf16[16,512,128]{1,2,0:T(8,128)(2,1)}), bf16[16,512,128]{1,2,0:T(8,128)(2,1)S(1)}, u32[]{:S(2)}, u32[]{:S(2)}) %all-to-all-start.2) | async-done | bytes 2097184 | tf_op jit(solution)/shard_map/all_to_all | solution.py:75
  135.7 1.1 stack.2
  136.8 5.8 %all-to-all-start = ((bf16[16,256,128]{1,2,0:T(8,128)(2,1)}), bf16[16,256,128]{1,2,0:T(8,128)(2,1)}, u32[]{:S(2)}, u32[]{:S(2)}) async-start(bf16[16,256,128]{1,2,0:T(8,128)(2,1)} %stack.2), calls=%async_computation | async-start | bytes 2097152 | tf_op jit(solution)/shard_map/all_to_all | solution.py:19
  142.9 2.5 %convolution_convert_fusion = bf16[512,128]{1,0:T(8,128)(2,1)} fusion(bf16[512,2048]{0,1:T(8,128)(2,1)S(1)} %bitcast.226, bf16[1,2048,128]{2,1,0:T(8,128)(2,1)} %param.31), kind=kOutput, calls=%fused_computation.42 | convolution fusion | flops 268500992 | bytes 2752512 | tf_op jit(solution)/shard_map/dot_general | solution.py:188
  145.3 25.4 %all-to-all-done = bf16[16,256,128]{1,2,0:T(8,128)(2,1)} async-done(((bf16[16,256,128]{1,2,0:T(8,128)(2,1)}), bf16[16,256,128]{1,2,0:T(8,128)(2,1)}, u32[]{:S(2)}, u32[]{:S(2)}) %all-to-all-start) | async-done | bytes 1048608 | tf_op jit(solution)/shard_map/all_to_all | solution.py:19
  170.7 5.8 %all-to-all-start.3 = ((bf16[32,16,128]{2,1,0:T(8,128)(2,1)}), bf16[32,16,128]{2,1,0:T(8,128)(2,1)S(1)}, u32[]{:S(2)}, u32[]{:S(2)}) async-start(bf16[32,16,128]{2,1,0:T(8,128)(2,1)} %bitcast.40), calls=%async_computation.3 | async-start | bytes 262144 | tf_op jit(solution)/shard_map/all_to_all | solution.py:192
  176.5 2.3 %convolution_convert_fusion.1 = bf16[256,128]{1,0:T(8,128)(2,1)} fusion(bf16[256,2048]{0,1:T(8,128)(2,1)} %bitcast.29, bf16[2048,128]{1,0:T(8,128)(2,1)S(1)} %copy-done.1), kind=kOutput, calls=%fused_computation.45 | convolution fusion | flops 134250496 | bytes 1638400 | tf_op jit(solution)/shard_map/dot_general | solution.py:168
  178.9 7.7 %all-to-all-done.3 = bf16[32,16,128]{2,1,0:T(8,128)(2,1)S(1)} async-done(((bf16[32,16,128]{2,1,0:T(8,128)(2,1)}), bf16[32,16,128]{2,1,0:T(8,128)(2,1)S(1)}, u32[]{:S(2)}, u32[]{:S(2)}) %all-to-all-start.3) | async-done | bytes 131104 | tf_op jit(solution)/shard_map/all_to_all | solution.py:192
  186.6 0.9 gather_fusion.1
  187.4 0.9 fusion.38
  (117 shorter events, 5.2 us)
Async XLA Ops:
  0.6 72.7 %copy-start = (bf16[1,2048,128]{2,1,0:T(8,128)(2,1)S(1)}, bf16[1,2048,128]{2,1,0:T(8,128)(2,1)}, u32[]{:S(2)}) copy-start(bf16[1,2048,128]{2,1,0:T(8,128)(2,1)} %param.29) | copy-start | bytes 1572868
  11.0 13.9 %copy-start.2 = (bf16[256,128]{1,0:T(8,128)(2,1)S(1)}, bf16[256,128]{1,0:T(8,128)(2,1)}, u32[]{:S(2)}) copy-start(bf16[256,128]{1,0:T(8,128)(2,1)} %param.19) | copy-start | bytes 196612
  11.0 13.9 %copy-start.11 = (f32[128]{0:T(128)S(1)}, f32[128]{0:T(128)}, u32[]{:S(2)}) copy-start(f32[128]{0:T(128)} %param.21) | copy-start | bytes 1540
  11.0 14.0 %copy-start.3 = (bf16[256,128]{1,0:T(8,128)(2,1)S(1)}, bf16[256,128]{1,0:T(8,128)(2,1)}, u32[]{:S(2)}) copy-start(bf16[256,128]{1,0:T(8,128)(2,1)} %param.17) | copy-start | bytes 196612
  11.0 14.0 %copy-start.4 = (bf16[256,128]{1,0:T(8,128)(2,1)S(1)}, bf16[256,128]{1,0:T(8,128)(2,1)}, u32[]{:S(2)}) copy-start(bf16[256,128]{1,0:T(8,128)(2,1)} %param.18) | copy-start | bytes 196612
  11.0 62.3 %all-to-all-start.1 = ((bf16[32,16,2048]{2,1,0:T(8,128)(2,1)}), bf16[32,16,2048]{2,1,0:T(8,128)(2,1)S(1)}, u32[]{:S(2)}, u32[]{:S(2)}) async-start(bf16[32,16,2048]{2,1,0:T(8,128)(2,1)} %bitcast.33), calls=%async_computation.1 | async-start | bytes 4194304 | tf_op jit(solution)/shard_map/all_to_all | solution.py:215
  73.3 1.0 copy-start.9
  76.8 9.9 %copy-start.10 = (f32[4,64,1,128]{3,1,2,0:T(8,128)S(1)}, f32[4,64,1,128]{3,1,2,0:T(8,128)}, u32[]{:S(2)}) copy-start(f32[4,64,1,128]{3,1,2,0:T(8,128)} %custom-call.7) | copy-start | bytes 393220
  76.8 58.9 %all-to-all-start.2 = ((bf16[16,512,128]{1,2,0:T(8,128)(2,1)}), bf16[16,512,128]{1,2,0:T(8,128)(2,1)S(1)}, u32[]{:S(2)}, u32[]{:S(2)}) async-start(bf16[16,512,128]{1,2,0:T(8,128)(2,1)} %broadcast_in_dim.37), calls=%async_computation.2 | async-start | bytes 4194304 | tf_op jit(solution)/shard_map/all_to_all | solution.py:75
  95.7 31.8 %copy-start.5 = (bf16[256,128]{1,0:T(8,128)(2,1)S(1)}, bf16[256,128]{1,0:T(8,128)(2,1)}, u32[]{:S(2)}) copy-start(bf16[256,128]{1,0:T(8,128)(2,1)} %param.20) | copy-start | bytes 196612
  95.7 31.8 %copy-start.8 = (f32[128]{0:T(128)S(1)}, f32[128]{0:T(128)}, u32[]{:S(2)}) copy-start(f32[128]{0:T(128)} %param.22) | copy-start | bytes 1540
  127.4 15.2 %copy-start.7 = (f32[128,2]{0,1:T(2,128)S(1)}, f32[128,2]{0,1:T(2,128)}, u32[]{:S(2)}) copy-start(f32[128,2]{0,1:T(2,128)} %param.28) | copy-start | bytes 3076
  127.4 15.2 %copy-start.6 = (f32[128,4]{0,1:T(4,128)S(1)}, f32[128,4]{0,1:T(4,128)}, u32[]{:S(2)}) copy-start(f32[128,4]{0,1:T(4,128)} %param.27) | copy-start | bytes 6148
  136.8 39.7 %copy-start.1 = (bf16[2048,128]{1,0:T(8,128)(2,1)S(1)}, bf16[2048,128]{1,0:T(8,128)(2,1)}, u32[]{:S(2)}) copy-start(bf16[2048,128]{1,0:T(8,128)(2,1)} %param.23) | copy-start | bytes 1572868
  136.8 33.9 %all-to-all-start = ((bf16[16,256,128]{1,2,0:T(8,128)(2,1)}), bf16[16,256,128]{1,2,0:T(8,128)(2,1)}, u32[]{:S(2)}, u32[]{:S(2)}) async-start(bf16[16,256,128]{1,2,0:T(8,128)(2,1)} %stack.2), calls=%async_computation | async-start | bytes 2097152 | tf_op jit(solution)/shard_map/all_to_all | solution.py:19
  170.7 15.8 %all-to-all-start.3 = ((bf16[32,16,128]{2,1,0:T(8,128)(2,1)}), bf16[32,16,128]{2,1,0:T(8,128)(2,1)S(1)}, u32[]{:S(2)}, u32[]{:S(2)}) async-start(bf16[32,16,128]{2,1,0:T(8,128)(2,1)} %bitcast.40), calls=%async_computation.3 | async-start | bytes 262144 | tf_op jit(solution)/shard_map/all_to_all | solution.py:192
